TPU v7x, 32 devices: a whole 2x2x4 slice. The times are simulated.
32 devices in a mesh: fs: 4 (over y, x), tp: 8 (over z, core).
Axes of the slice: x: 2, y: 2, z: 4, core: 2. Of those that a mesh axis runs over, the one named last changes fastest.
Arguments:
- normed_inputs: bfloat16 [4096, 4096], P('fs', 'tp'), may hold values from -6 to 6
- query_upstream: bfloat16 [4096, 4096], P('fs', 'tp'), may hold values from -0.125 to 0.125
- key_upstream: bfloat16 [4096, 1024], P('fs', 'tp'), may hold values from -0.09375 to 0.09375
- head_outputs: bfloat16 [4096, 4096], P('fs', 'tp'), may hold values from -6 to 6
- branch_upstream: bfloat16 [4096, 4096], P('fs', 'tp'), may hold values from -0.125 to 0.125
- query_master: float32 [4096, 4096], P('fs', 'tp'), may hold values from -0.09375 to 0.09375
- key_master: float32 [4096, 1024], P('fs', 'tp'), may hold values from -0.09375 to 0.09375
- branch_master: float32 [4096, 4096], P('fs', 'tp'), may hold values from -0.09375 to 0.09375
- query_basis: bfloat16 [4096, 128], replicated, may hold values from -0.09375 to 0.09375
- key_basis: bfloat16 [4096, 128], replicated, may hold values from -0.09375 to 0.09375
- branch_basis: bfloat16 [4096, 128], replicated, may hold values from -0.09375 to 0.09375
- query_first: float32 [128, 4096], P(None, 'tp'), may hold values from -0.75 to 0.75
- query_second: float32 [128, 4096], P(None, 'tp'), may hold values from 0.001 to 0.02
- key_first: float32 [128, 1024], P(None, 'tp'), may hold values from -0.75 to 0.75
- key_second: float32 [128, 1024], P(None, 'tp'), may hold values from 0.001 to 0.02
- branch_first: float32 [4096, 128], P('fs'), may hold values from -0.75 to 0.75
- branch_second: float32 [4096, 128], P('fs'), may hold values from 0.001 to 0.02
Outputs:
- query_step: float32 [4096, 4096], P('fs', 'tp')
- key_step: float32 [4096, 1024], P('fs', 'tp')
- branch_step: float32 [4096, 4096], P('fs', 'tp')
- query_updated: float32 [4096, 4096], P('fs', 'tp')
- key_updated: float32 [4096, 1024], P('fs', 'tp')
- branch_updated: float32 [4096, 4096], P('fs', 'tp')
- query_copy: bfloat16 [4096, 4096], P(None, 'tp')
- key_copy: bfloat16 [4096, 1024], P(None, 'tp')
- branch_copy: bfloat16 [4096, 4096], P(None, 'tp')
- query_first_new: float32 [128, 4096], P(None, 'tp')
- query_second_new: float32 [128, 4096], P(None, 'tp')
- key_first_new: float32 [128, 1024], P(None, 'tp')
- key_second_new: float32 [128, 1024], P(None, 'tp')
- branch_first_new: float32 [4096, 128], P('fs')
- branch_second_new: float32 [4096, 128], P('fs')
All inputs are finite; a program needn't handle non-finite values.
Results may differ from a plain program's by a relative error of at most 0.001.
Values may be sent and summed in bfloat16 or wider, within the bound.
No kernel may reach another device: no remote copies, remote signals or barrier semaphores. Data moves between devices by JAX's collectives and lax.ppermute only.
A program may use at most 128 MiB of HBM per device.

v0:
```python
import jax
import jax.numpy as jnp
from jax import lax
from jax.sharding import PartitionSpec as P

LEARN = 0.02
BETA_ONE = 0.9
BETA_TWO = 0.95
ADAM_EPS = 1e-08
CLIP_RMS = 0.5


def moments(first, second, low, clip):
    scaled = clip * low
    first_new = BETA_ONE * first + (1.0 - BETA_ONE) * scaled
    second_new = BETA_TWO * second + (1.0 - BETA_TWO) * scaled * scaled
    return (first_new, second_new, first_new / (jnp.sqrt(second_new) + ADAM_EPS))


def over_tokens(left, right, precision=None):
    return lax.dot_general(
        left,
        right,
        (((0,), (0,)), ((), ())),
        precision=precision,
        preferred_element_type=jnp.float32,
    )


def per_device(
    normed_inputs,
    query_upstream,
    key_upstream,
    head_outputs,
    branch_upstream,
    query_master,
    key_master,
    branch_master,
    query_basis,
    key_basis,
    branch_basis,
    query_first,
    query_second,
    key_first,
    key_second,
    branch_first,
    branch_second,
):
    exact = lax.Precision.HIGHEST
    row_index = lax.axis_index("fs")
    col_index = lax.axis_index("tp")
    n_rows = lax.axis_size("fs")
    n_cols = lax.axis_size("tp")
    features = normed_inputs.shape[1]
    query_local = query_upstream.shape[1]
    key_local = key_upstream.shape[1]
    rows_in = query_master.shape[0]
    rank = query_basis.shape[1]
    whole_values = lax.all_gather(head_outputs, "tp", axis=1, tiled=True)
    block_query = lax.dynamic_slice_in_dim(query_basis, col_index * features, features, 0)
    block_key = lax.dynamic_slice_in_dim(key_basis, col_index * features, features, 0)
    proj_query, proj_key = lax.psum(
        (
            jnp.dot(normed_inputs, block_query, preferred_element_type=jnp.float32),
            jnp.dot(normed_inputs, block_key, preferred_element_type=jnp.float32),
        ),
        "tp",
    )
    part_query = over_tokens(proj_query, query_upstream.astype(jnp.float32), exact)
    part_key = over_tokens(proj_key, key_upstream.astype(jnp.float32), exact)
    grad_branch = lax.psum_scatter(
        over_tokens(whole_values, branch_upstream), "fs", scatter_dimension=0, tiled=True
    )
    own_branch = lax.dynamic_slice_in_dim(branch_basis, col_index * features, features, 0).astype(
        jnp.float32
    )
    part_branch = jnp.dot(grad_branch, own_branch, precision=exact)
    query_low, key_low = lax.psum((part_query, part_key), "fs")
    branch_low = lax.psum(part_branch, "tp")
    local_squares = (jnp.sum(query_low * query_low) + jnp.sum(key_low * key_low)) / n_rows
    local_squares = local_squares + jnp.sum(branch_low * branch_low) / n_cols
    total = lax.psum(local_squares, ("fs", "tp"))
    entries = rank * n_cols * (2 * query_local + key_local)
    rms_value = jnp.sqrt(total / float(entries))
    clip = 1.0 / jnp.maximum(1.0, rms_value / CLIP_RMS)
    q_first, q_second, q_dir = moments(query_first, query_second, query_low, clip)
    k_first, k_second, k_dir = moments(key_first, key_second, key_low, clip)
    b_first, b_second, b_dir = moments(branch_first, branch_second, branch_low, clip)
    step_rows_query = lax.dynamic_slice_in_dim(query_basis, row_index * rows_in, rows_in, 0).astype(
        jnp.float32
    )
    step_rows_key = lax.dynamic_slice_in_dim(key_basis, row_index * rows_in, rows_in, 0).astype(
        jnp.float32
    )
    query_step = jnp.dot(step_rows_query, q_dir, precision=exact)
    key_step = jnp.dot(step_rows_key, k_dir, precision=exact)
    branch_step = jnp.dot(b_dir, own_branch.T, precision=exact)
    query_updated = query_master - LEARN * query_step
    key_updated = key_master - LEARN * key_step
    branch_updated = branch_master - LEARN * branch_step
    query_copy, key_copy, branch_copy = (
        lax.all_gather(query_updated.astype(jnp.bfloat16), "fs", axis=0, tiled=True),
        lax.all_gather(key_updated.astype(jnp.bfloat16), "fs", axis=0, tiled=True),
        lax.all_gather(branch_updated.astype(jnp.bfloat16), "fs", axis=0, tiled=True),
    )
    return (
        query_step,
        key_step,
        branch_step,
        query_updated,
        key_updated,
        branch_updated,
        query_copy,
        key_copy,
        branch_copy,
        q_first,
        q_second,
        k_first,
        k_second,
        b_first,
        b_second,
    )


def solution(mesh):
    return jax.shard_map(
        per_device,
        mesh=mesh,
        in_specs=(
            P("fs", "tp"),
            P("fs", "tp"),
            P("fs", "tp"),
            P("fs", "tp"),
            P("fs", "tp"),
            P("fs", "tp"),
            P("fs", "tp"),
            P("fs", "tp"),
            P(),
            P(),
            P(),
            P(None, "tp"),
            P(None, "tp"),
            P(None, "tp"),
            P(None, "tp"),
            P("fs", None),
            P("fs", None),
        ),
        out_specs=(
            P("fs", "tp"),
            P("fs", "tp"),
            P("fs", "tp"),
            P("fs", "tp"),
            P("fs", "tp"),
            P("fs", "tp"),
            P(None, "tp"),
            P(None, "tp"),
            P(None, "tp"),
            P(None, "tp"),
            P(None, "tp"),
            P(None, "tp"),
            P(None, "tp"),
            P("fs", None),
            P("fs", None),
        ),
        check_vma=False,
    )
```

profile of v0, /device:TPU:0, one launch (start us, length us, event | category | flops | bytes accessed | tf_op | source)
XLA Modules:
  0.0 502.3 jit_solution(1356573704103843505)
XLA Ops:
  8.0 86.4 %all-gather.5.cloned.1.call-done = bf16[1024,4096]{1,0:T(8,128)(2,1)} async-done(((bf16[1024,512]{1,0:T(8,128)(2,1)}), bf16[1024,4096]{1,0:T(8,128)(2,1)}) %all-gather.5.cloned.1.call-update) | async-done | bytes 8388624 | tf_op jit(solution)/shard_map/all_gather | solution.py:59
  94.4 10.4 %fusion.39 = f32[4096,512]{1,0:T(8,128)} fusion(bf16[1024,4096]{1,0:T(8,128)(2,1)} %all-gather.5.cloned.1.call-done, bf16[1024,512]{1,0:T(8,128)(2,1)S(1)} %copy-done), kind=kOutput, calls=%fused_computation.53 | convolution fusion | flops 4294967296 | bytes 17825792 | tf_op jit(solution)/shard_map/dot_general | solution.py:21
  104.9 1.1 copy-done.2
  106.1 2.2 convolution_bitcast_fusion
  108.2 2.2 convolution_bitcast_fusion.1
  110.4 79.4 %reduce-scatter.2.cloned.1.call-done = f32[1024,512]{1,0:T(8,128)} async-done(((f32[4096,512]{1,0:T(8,128)}), f32[1024,512]{1,0:T(8,128)}) %reduce-scatter.2.cloned.1.call-update) | async-done | bytes 2097168 | tf_op jit(solution)/shard_map/reduce_scatter | solution.py:71
  189.8 3.4 fusion.18
  193.4 62.4 %all-reduce.5.cloned.1.call-done = (f32[1024,128]{0,1:T(8,128)}, f32[1024,128]{0,1:T(8,128)}, f32[1024,128]{1,0:T(8,128)}) async-done(((f32[1024,128]{0,1:T(8,128)}, f32[1024,128]{0,1:T(8,128)}, f32[1024,128]{1,0:T(8,128)}), (f32[1024,128]{0,1:T(8,128)}, f32[1024,128]{0,1:T(8,128)}, f32[1024,128]{1,0:T(8,128)})) %all-reduce.5.cloned.1.call-update) | async-done | bytes 1572880 | tf_op jit(solution)/shard_map/psum | solution.py:62
  255.8 2.5 fusion.37
  258.3 1.0 fusion.38
  260.7 41.6 %all-reduce.7.cloned.1.call-done = (f32[128,512]{1,0:T(8,128)}, f32[128,128]{1,0:T(8,128)}) async-done(((f32[128,512]{1,0:T(8,128)}, f32[128,128]{1,0:T(8,128)}), (f32[128,512]{1,0:T(8,128)}, f32[128,128]{1,0:T(8,128)})) %all-reduce.7.cloned.1.call-update) | async-done | bytes 327696 | tf_op jit(solution)/shard_map/psum | solution.py:78
  302.3 1.6 multiply_reduce_fusion.1
  303.9 1.5 multiply_reduce_fusion.2
  306.7 39.3 %psum.47 = f32[]{:T(128)} all-reduce(f32[]{:T(128)S(6)} %add.68), channel_id=1, replica_groups=mesh['fs'=4,'tp'=8] {'fs','tp'}, use_global_device_ids=true, to_apply=%region_9.0 | all-reduce | flops 1 | bytes 8 | tf_op jit(solution)/shard_map/psum | solution.py:82
  347.7 2.6 fusion.35
  350.3 1.4 fusion
  351.7 4.7 fusion.34
  356.5 1.2 fusion.5
  358.1 4.5 fusion.36
  362.7 15.2 %all-gather.9.cloned.1.call-done = bf16[4096,128]{1,0:T(8,128)(2,1)} async-done(((bf16[1024,128]{1,0:T(8,128)(2,1)}), bf16[4096,128]{1,0:T(8,128)(2,1)}) %all-gather.9.cloned.1.call-update) | async-done | bytes 1048592 | tf_op jit(solution)/shard_map/all_gather | solution.py:103
  377.9 54.9 %all-gather.11.cloned.1.call-done = bf16[4096,512]{1,0:T(8,128)(2,1)} async-done(((bf16[1024,512]{1,0:T(8,128)(2,1)}), bf16[4096,512]{1,0:T(8,128)(2,1)}) %all-gather.11.cloned.1.call-update) | async-done | bytes 4194320 | tf_op jit(solution)/shard_map/all_gather | solution.py:104
  432.8 55.0 %all-gather.7.cloned.1.call-done = bf16[4096,512]{1,0:T(8,128)(2,1)} async-done(((bf16[1024,512]{1,0:T(8,128)(2,1)}), bf16[4096,512]{1,0:T(8,128)(2,1)}) %all-gather.7.cloned.1.call-update) | async-done | bytes 4194320 | tf_op jit(solution)/shard_map/all_gather | solution.py:102
  487.8 4.6 copy.40
  493.4 2.0 copy.42
  (60 shorter events, 4.2 us)
Async XLA Ops:
  7.2 87.2 %copy-start = (bf16[1024,512]{1,0:T(8,128)(2,1)S(1)}, bf16[1024,512]{1,0:T(8,128)(2,1)}, u32[]{:S(2)}) copy-start(bf16[1024,512]{1,0:T(8,128)(2,1)} %param.21) | copy-start | bytes 3145732
  7.2 87.2 %all-gather.5.cloned.1.call-start = ((), (), s32[]{:S(2)}) async-start(), calls=%async_computation.1 | async-start | bytes 9437184 | tf_op jit(solution)/shard_map/all_gather | solution.py:59
  7.9 181.9 %reduce-scatter.2.cloned.1.call-start = ((), (), s32[]{:S(2)}) async-start(), calls=%async_computation.2 | async-start | bytes 10485760 | tf_op jit(solution)/shard_map/reduce_scatter | solution.py:71
  104.9 150.9 %all-reduce.5.cloned.1.call-start = ((), (), s32[]{:S(2)}) async-start(), calls=%async_computation.6 | async-start | bytes 3145728 | tf_op jit(solution)/shard_map/psum | solution.py:62
  110.4 145.4 %copy-start.11 = (bf16[1024,512]{1,0:T(8,128)(2,1)S(1)}, bf16[1024,512]{1,0:T(8,128)(2,1)}, u32[]{:S(2)}) copy-start(bf16[1024,512]{1,0:T(8,128)(2,1)} %param.18) | copy-start | bytes 3145732
  193.3 65.0 %copy-start.19 = (bf16[1024,128]{1,0:T(8,128)(2,1)S(1)}, bf16[1024,128]{1,0:T(8,128)(2,1)}, u32[]{:S(2)}) copy-start(bf16[1024,128]{1,0:T(8,128)(2,1)} %param.19) | copy-start | bytes 786436
  193.3 153.5 %copy-start.20 = (f32[128,128]{1,0:T(8,128)S(1)}, f32[128,128]{1,0:T(8,128)}, u32[]{:S(2)}) copy-start(f32[128,128]{1,0:T(8,128)} %param.31) | copy-start | bytes 196612
  193.3 153.5 %copy-start.21 = (f32[128,128]{1,0:T(8,128)S(1)}, f32[128,128]{1,0:T(8,128)}, u32[]{:S(2)}) copy-start(f32[128,128]{1,0:T(8,128)} %param.30) | copy-start | bytes 196612
  193.3 109.0 %all-reduce.7.cloned.1.call-start = ((), (), s32[]{:S(2)}) async-start(), calls=%async_computation.7 | async-start | bytes 655360 | tf_op jit(solution)/shard_map/psum | solution.py:78
  255.8 91.9 %copy-start.14 = (f32[1024,128]{1,0:T(8,128)S(1)}, f32[1024,128]{1,0:T(8,128)}, u32[]{:S(2)}) copy-start(f32[1024,128]{1,0:T(8,128)} %param.23) | copy-start | bytes 1572868
  259.3 118.6 %all-gather.9.cloned.1.call-start = ((), (), s32[]{:S(2)}) async-start(), calls=%async_computation.4 | async-start | bytes 1310720 | tf_op jit(solution)/shard_map/all_gather | solution.py:103
  347.6 4.0 copy-start.17
  347.6 4.0 copy-start.18
  347.7 4.0 copy-start.7
  350.3 82.5 %all-gather.11.cloned.1.call-start = ((), (), s32[]{:S(2)}) async-start(), calls=%async_computation.5 | async-start | bytes 5242880 | tf_op jit(solution)/shard_map/all_gather | solution.py:104
  351.7 4.7 copy-start.4
  351.7 4.7 copy-start.5
  351.7 4.8 copy-start.12
  351.7 4.8 copy-start.16
  356.4 131.4 %all-gather.7.cloned.1.call-start = ((), (), s32[]{:S(2)}) async-start(), calls=%async_computation.3 | async-start | bytes 5242880 | tf_op jit(solution)/shard_map/all_gather | solution.py:102
  357.7 5.0 copy-start.9
  357.7 5.0 copy-start.10
  487.8 4.6 copy-start.13
  487.8 5.6 %copy-start.3 = (bf16[4096,512]{1,0:T(8,128)(2,1)S(1)}, bf16[4096,512]{1,0:T(8,128)(2,1)}, u32[]{:S(2)}) copy-start(bf16[4096,512]{1,0:T(8,128)(2,1)} %all-gather.11.cloned.1.call-done) | copy-start | bytes 12582916
  (5 other events, 11.0 us)
Sparse Core Ops, SparseCore 0:
  9.6 84.7 all-gather.4
  105.0 84.7 reduce-scatter.1
  193.6 62.1 all-reduce.4
  259.4 42.8 all-reduce.6
  350.4 27.4 all-gather.8
  380.2 52.5 all-gather.10
  435.2 52.5 all-gather.6
where the time goes:
time: 503 us; the launch traced here: 502 us
  waiting for transfers between devices  396 us (79%)
  blocking collectives  39.3 us (8%)
  matrix products  33.4 us (7%)
  between operations  17 us (3%)
  local copies, waits for them, and re-layouts  9.28 us (2%)
  other arithmetic  7.2 us (1%)
    all_gather x1, waiting for transfers between devices, per_device(): whole_values = lax.all_gather(head_outputs, 'tp', axis=1, tiled=True)  86.4 us
    reduce_scatter x1, waiting for transfers between devices, per_device(): lax.psum_scatter(over_tokens(whole_values, branch_upstream), 'fs', scatte...  79.4 us
    psum x1, waiting for transfers between devices, per_device(): lax.psum((jnp.dot(normed_inputs, block_query, preferred_element_type=jnp....  62.4 us
    all_gather x1, waiting for transfers between devices, per_device(): lax.all_gather(query_updated.astype(jnp.bfloat16), 'fs', axis=0, tiled=True)  55 us
    all_gather x1, waiting for transfers between devices, per_device(): lax.all_gather(branch_updated.astype(jnp.bfloat16), 'fs', axis=0, tiled=T...  54.9 us
    psum x1, waiting for transfers between devices, per_device(): query_low, key_low = lax.psum((part_query, part_key), 'fs')  41.6 us
    psum x1, blocking collectives, per_device(): total = lax.psum(local_squares, ('fs', 'tp'))  39.3 us
    all_gather x1, waiting for transfers between devices, per_device(): lax.all_gather(key_updated.astype(jnp.bfloat16), 'fs', axis=0, tiled=True)  15.2 us
  transfers between devices with their start and end apart: 7, of which 7 were waited for; matrix products, arithmetic and copies ran while one was open for 3% of the time, Pallas kernels for 0%

commit v1 on v0

--- a/solution.py
+++ b/solution.py
@@ -1,3 +1,4 @@
+import functools
 import jax
 import jax.numpy as jnp
 from jax import lax
@@ -8,6 +9,15 @@
 BETA_TWO = 0.95
 ADAM_EPS = 1e-08
 CLIP_RMS = 0.5
+
+
+def lift_paths_in(vec, mesh_name, bus_axis):
+    for tick in (mesh_name, bus_axis):
+        vec = lax.psum(vec, axis_name=tick)
+    return vec
+
+
+end_groups = functools.partial(lift_paths_in, mesh_name="tp", bus_axis="fs")
 
 
 def moments(first, second, low, clip):
@@ -79,7 +89,7 @@
     branch_low = lax.psum(part_branch, "tp")
     local_squares = (jnp.sum(query_low * query_low) + jnp.sum(key_low * key_low)) / n_rows
     local_squares = local_squares + jnp.sum(branch_low * branch_low) / n_cols
-    total = lax.psum(local_squares, ("fs", "tp"))
+    total = end_groups(local_squares)
     entries = rank * n_cols * (2 * query_local + key_local)
     rms_value = jnp.sqrt(total / float(entries))
     clip = 1.0 / jnp.maximum(1.0, rms_value / CLIP_RMS)

time: 503 us -> 486 us (0.966)
  blocking collectives: 39.3 us -> 25.9 us
    psum x1 -> x2, blocking collectives: 39.3 us -> 25.9 us  [lift_paths_in(): vec = lax.psum(vec, axis_name=tick)]
where the time goes in v1:
time: 486 us; the launch traced here: 485 us
  waiting for transfers between devices  392 us (81%)
  matrix products  33.4 us (7%)
  blocking collectives  25.9 us (5%)
  between operations  17 us (3%)
  local copies, waits for them, and re-layouts  9.24 us (2%)
  other arithmetic  7.2 us (1%)
    all_gather x1, waiting for transfers between devices, per_device(): whole_values = lax.all_gather(head_outputs, 'tp', axis=1, tiled=True)  86.4 us
    reduce_scatter x1, waiting for transfers between devices, per_device(): lax.psum_scatter(over_tokens(whole_values, branch_upstream), 'fs', scatte...  79.4 us
    psum x1, waiting for transfers between devices, per_device(): lax.psum((jnp.dot(normed_inputs, block_query, preferred_element_type=jnp....  62.4 us
    all_gather x1, waiting for transfers between devices, per_device(): lax.all_gather(query_updated.astype(jnp.bfloat16), 'fs', axis=0, tiled=True)  55 us
    all_gather x1, waiting for transfers between devices, per_device(): lax.all_gather(branch_updated.astype(jnp.bfloat16), 'fs', axis=0, tiled=T...  54.9 us
    psum x1, waiting for transfers between devices, per_device(): query_low, key_low = lax.psum((part_query, part_key), 'fs')  41.6 us
    psum x2, blocking collectives, lift_paths_in(): vec = lax.psum(vec, axis_name=tick)  25.9 us
    dot_general x3, matrix products, over_tokens(): lax.dot_general(left, right, (((0,), (0,)), ((), ())), precision=precisio...  13.9 us
  transfers between devices with their start and end apart: 7, of which 7 were waited for; matrix products, arithmetic and copies ran while one was open for 3% of the time, Pallas kernels for 0%

profile of v1, /device:TPU:0, one launch (start us, length us, event | category | flops | bytes accessed | tf_op | source)
XLA Modules:
  0.0 485.1 jit_solution(5154986880827905871)
XLA Ops:
  8.0 86.4 %all-gather.5.cloned.1.call-done = bf16[1024,4096]{1,0:T(8,128)(2,1)} async-done(((bf16[1024,512]{1,0:T(8,128)(2,1)}), bf16[1024,4096]{1,0:T(8,128)(2,1)}) %all-gather.5.cloned.1.call-update) | async-done | bytes 8388624 | tf_op jit(solution)/shard_map/all_gather | solution.py:69
  94.4 10.5 %fusion.39 = f32[4096,512]{1,0:T(8,128)} fusion(bf16[1024,4096]{1,0:T(8,128)(2,1)} %all-gather.5.cloned.1.call-done, bf16[1024,512]{1,0:T(8,128)(2,1)S(1)} %copy-done), kind=kOutput, calls=%fused_computation.53 | convolution fusion | flops 4294967296 | bytes 17825792 | tf_op jit(solution)/shard_map/dot_general | solution.py:31
  104.9 1.1 copy-done.2
  106.1 2.2 convolution_bitcast_fusion
  108.3 2.2 convolution_bitcast_fusion.1
  110.4 79.4 %reduce-scatter.2.cloned.1.call-done = f32[1024,512]{1,0:T(8,128)} async-done(((f32[4096,512]{1,0:T(8,128)}), f32[1024,512]{1,0:T(8,128)}) %reduce-scatter.2.cloned.1.call-update) | async-done | bytes 2097168 | tf_op jit(solution)/shard_map/reduce_scatter | solution.py:81
  189.8 3.4 fusion.18
  193.4 62.4 %all-reduce.5.cloned.1.call-done = (f32[1024,128]{0,1:T(8,128)}, f32[1024,128]{0,1:T(8,128)}, f32[1024,128]{1,0:T(8,128)}) async-done(((f32[1024,128]{0,1:T(8,128)}, f32[1024,128]{0,1:T(8,128)}, f32[1024,128]{1,0:T(8,128)}), (f32[1024,128]{0,1:T(8,128)}, f32[1024,128]{0,1:T(8,128)}, f32[1024,128]{1,0:T(8,128)})) %all-reduce.5.cloned.1.call-update) | async-done | bytes 1572880 | tf_op jit(solution)/shard_map/psum | solution.py:72
  255.8 2.5 fusion.37
  260.8 41.6 %all-reduce.7.cloned.1.call-done = (f32[128,512]{1,0:T(8,128)}, f32[128,128]{1,0:T(8,128)}) async-done(((f32[128,512]{1,0:T(8,128)}, f32[128,128]{1,0:T(8,128)}), (f32[128,512]{1,0:T(8,128)}, f32[128,128]{1,0:T(8,128)})) %all-reduce.7.cloned.1.call-update) | async-done | bytes 327696 | tf_op jit(solution)/shard_map/psum | solution.py:88
  302.3 1.6 multiply_reduce_fusion.1
  303.9 1.5 multiply_reduce_fusion.2
  306.7 16.4 %psum.54 = f32[]{:T(128)} all-reduce(f32[]{:T(128)S(6)} %add.70), channel_id=1, replica_groups=mesh['fs'=4,'tp'=8] {'tp'}, use_global_device_ids=true, to_apply=%region_9.0 | all-reduce | flops 1 | bytes 8 | tf_op jit(solution)/shard_map/psum | solution.py:16
  323.1 9.5 %psum.55 = f32[]{:T(128)} all-reduce(f32[]{:T(128)} %psum.54), channel_id=1, replica_groups=mesh['fs'=4,'tp'=8] {'fs'}, use_global_device_ids=true, to_apply=%region_10.0 | all-reduce | flops 1 | bytes 8 | tf_op jit(solution)/shard_map/psum | solution.py:16
  334.3 2.6 fusion.35
  336.9 1.4 fusion
  338.3 4.7 fusion.34
  343.1 1.2 fusion.5
  344.7 4.5 fusion.36
  349.2 11.5 %all-gather.9.cloned.1.call-done = bf16[4096,128]{1,0:T(8,128)(2,1)} async-done(((bf16[1024,128]{1,0:T(8,128)(2,1)}), bf16[4096,128]{1,0:T(8,128)(2,1)}) %all-gather.9.cloned.1.call-update) | async-done | bytes 1048592 | tf_op jit(solution)/shard_map/all_gather | solution.py:113
  360.7 54.9 %all-gather.11.cloned.1.call-done = bf16[4096,512]{1,0:T(8,128)(2,1)} async-done(((bf16[1024,512]{1,0:T(8,128)(2,1)}), bf16[4096,512]{1,0:T(8,128)(2,1)}) %all-gather.11.cloned.1.call-update) | async-done | bytes 4194320 | tf_op jit(solution)/shard_map/all_gather | solution.py:114
  415.6 55.0 %all-gather.7.cloned.1.call-done = bf16[4096,512]{1,0:T(8,128)(2,1)} async-done(((bf16[1024,512]{1,0:T(8,128)(2,1)}), bf16[4096,512]{1,0:T(8,128)(2,1)}) %all-gather.7.cloned.1.call-update) | async-done | bytes 4194320 | tf_op jit(solution)/shard_map/all_gather | solution.py:112
  470.6 4.6 copy.40
  476.2 2.0 copy.42
  (61 shorter events, 5.1 us)
Async XLA Ops:
  7.2 87.2 %copy-start = (bf16[1024,512]{1,0:T(8,128)(2,1)S(1)}, bf16[1024,512]{1,0:T(8,128)(2,1)}, u32[]{:S(2)}) copy-start(bf16[1024,512]{1,0:T(8,128)(2,1)} %param.21) | copy-start | bytes 3145732
  7.2 87.2 %all-gather.5.cloned.1.call-start = ((), (), s32[]{:S(2)}) async-start(), calls=%async_computation.1 | async-start | bytes 9437184 | tf_op jit(solution)/shard_map/all_gather | solution.py:69
  7.9 181.9 %reduce-scatter.2.cloned.1.call-start = ((), (), s32[]{:S(2)}) async-start(), calls=%async_computation.2 | async-start | bytes 10485760 | tf_op jit(solution)/shard_map/reduce_scatter | solution.py:81
  104.9 150.9 %all-reduce.5.cloned.1.call-start = ((), (), s32[]{:S(2)}) async-start(), calls=%async_computation.6 | async-start | bytes 3145728 | tf_op jit(solution)/shard_map/psum | solution.py:72
  110.4 145.4 %copy-start.11 = (bf16[1024,512]{1,0:T(8,128)(2,1)S(1)}, bf16[1024,512]{1,0:T(8,128)(2,1)}, u32[]{:S(2)}) copy-start(bf16[1024,512]{1,0:T(8,128)(2,1)} %param.18) | copy-start | bytes 3145732
  193.3 65.0 %copy-start.19 = (bf16[1024,128]{1,0:T(8,128)(2,1)S(1)}, bf16[1024,128]{1,0:T(8,128)(2,1)}, u32[]{:S(2)}) copy-start(bf16[1024,128]{1,0:T(8,128)(2,1)} %param.19) | copy-start | bytes 786436
  193.3 140.0 %copy-start.20 = (f32[128,128]{1,0:T(8,128)S(1)}, f32[128,128]{1,0:T(8,128)}, u32[]{:S(2)}) copy-start(f32[128,128]{1,0:T(8,128)} %param.31) | copy-start | bytes 196612
  193.3 140.0 %copy-start.21 = (f32[128,128]{1,0:T(8,128)S(1)}, f32[128,128]{1,0:T(8,128)}, u32[]{:S(2)}) copy-start(f32[128,128]{1,0:T(8,128)} %param.30) | copy-start | bytes 196612
  193.3 109.0 %all-reduce.7.cloned.1.call-start = ((), (), s32[]{:S(2)}) async-start(), calls=%async_computation.7 | async-start | bytes 655360 | tf_op jit(solution)/shard_map/psum | solution.py:88
  255.8 78.4 %copy-start.14 = (f32[1024,128]{1,0:T(8,128)S(1)}, f32[1024,128]{1,0:T(8,128)}, u32[]{:S(2)}) copy-start(f32[1024,128]{1,0:T(8,128)} %param.23) | copy-start | bytes 1572868
  259.3 101.4 %all-gather.9.cloned.1.call-start = ((), (), s32[]{:S(2)}) async-start(), calls=%async_computation.4 | async-start | bytes 1310720 | tf_op jit(solution)/shard_map/all_gather | solution.py:113
  334.2 4.0 copy-start.17
  334.2 4.0 copy-start.18
  334.3 4.0 copy-start.7
  336.8 78.7 %all-gather.11.cloned.1.call-start = ((), (), s32[]{:S(2)}) async-start(), calls=%async_computation.5 | async-start | bytes 5242880 | tf_op jit(solution)/shard_map/all_gather | solution.py:114
  338.3 4.7 copy-start.4
  338.3 4.7 copy-start.5
  338.3 4.8 copy-start.12
  338.3 4.8 copy-start.16
  343.0 127.6 %all-gather.7.cloned.1.call-start = ((), (), s32[]{:S(2)}) async-start(), calls=%async_computation.3 | async-start | bytes 5242880 | tf_op jit(solution)/shard_map/all_gather | solution.py:112
  344.3 4.9 %copy-start.9 = (f32[128,512]{1,0:T(8,128)}, f32[128,512]{1,0:T(8,128)S(1)}, u32[]{:S(2)}) copy-start(f32[128,512]{1,0:T(8,128)S(1)} %get-tuple-element.60) | copy-start | bytes 786436
  344.3 4.9 %copy-start.10 = (f32[128,512]{1,0:T(8,128)}, f32[128,512]{1,0:T(8,128)S(1)}, u32[]{:S(2)}) copy-start(f32[128,512]{1,0:T(8,128)S(1)} %get-tuple-element.59) | copy-start | bytes 786436
  470.6 4.6 copy-start.13
  470.6 5.6 %copy-start.3 = (bf16[4096,512]{1,0:T(8,128)(2,1)S(1)}, bf16[4096,512]{1,0:T(8,128)(2,1)}, u32[]{:S(2)}) copy-start(bf16[4096,512]{1,0:T(8,128)(2,1)} %all-gather.11.cloned.1.call-done) | copy-start | bytes 12582916
  (5 other events, 10.9 us)
Sparse Core Ops, SparseCore 0:
  9.6 84.7 all-gather.4
  105.0 84.7 reduce-scatter.1
  193.6 62.1 all-reduce.4
  259.4 42.8 all-reduce.6
  337.0 23.6 all-gather.8
  363.0 52.5 all-gather.10
  418.0 52.5 all-gather.6
